TPU v7x, 32 devices: a whole 2x2x4 slice. The times are simulated.
32 devices in a mesh: gr: 2 (over x), sp: 8 (over z, y), tp: 2 (over core).
Axes of the slice: x: 2, y: 2, z: 4, core: 2. Of those that a mesh axis runs over, the one named last changes fastest.
Arguments:
- prompt_block_input: bfloat16 [16, 2048, 2048], P('gr', 'sp'), may hold values from -6 to 6
- key_projection_weight: bfloat16 [2048, 512], P(None, 'tp'), may hold values from -0.125 to 0.125
- value_projection_weight: bfloat16 [2048, 512], P(None, 'tp'), may hold values from -0.125 to 0.125
- forget_gate_weight: bfloat16 [8, 2048], P('tp'), may hold values from -0.125 to 0.125
- forget_gate_bias: float32 [8], P('tp'), may hold values from 3.5 to 12
- forget_gate_scale: float32 [16, 8, 2048], P('gr', 'tp', 'sp'), may hold values from 0.15 to 6
- gate_spike_added: float32 [16, 8, 2048], P('gr', 'tp', 'sp'), may hold values from -0.7 to 0
- prior_key_value_cache: bfloat16 [16, 14336, 8, 128], P(('gr', 'sp'), None, 'tp')
- prior_cumulative_log_forget: float32 [16, 8, 14336], P(('gr', 'sp'), 'tp'), as said below
- decoded_token_query: bfloat16 [16, 1024], P('gr', 'tp')
- decoded_token_key: bfloat16 [16, 512], P(('gr', 'sp'), 'tp'), may hold values from -6 to 6
- decoded_token_value: bfloat16 [16, 512], P(('gr', 'sp'), 'tp'), may hold values from -6 to 6
- decoded_log_gate: float32 [16, 8], P(('gr', 'sp'), 'tp'), may hold values from -2.5 to -0.05
- key_norm_gain: float32 [64], replicated, may hold values from 0.1 to 1.9
- read_norm_gain: float32 [1024], P('tp'), may hold values from 0.1 to 1.9
Outputs:
- new_cache: bfloat16 [16, 2048, 8, 128], P(('gr', 'sp'), None, 'tp')
- new_logc: float32 [16, 8, 2048], P(('gr', 'sp'), 'tp')
- next_read: bfloat16 [16, 1024], P(('gr', 'sp'), 'tp')
Inputs may be any that keep to these rules, and one draw needn't show every extreme that they name: `prior_cumulative_log_forget`: each position's cumulative log forget value from the start of its sequence.
All inputs are finite; a program needn't handle non-finite values.
Results may differ from a plain program's by a relative error of at most 0.008.
Values may be sent and summed in bfloat16 or wider, within the bound.
A program may use at most 128 MiB of HBM per device.

v0:
```python
import jax
import jax.numpy as jnp
from jax import lax
from jax.sharding import PartitionSpec as P

EPSILON = 1e-06


def project(
    tok_rows,
    key_projection_weight,
    value_projection_weight,
    forget_gate_weight,
    forget_gate_bias,
    key_norm_gain,
):
    head_dim = key_norm_gain.shape[0]
    key_raw = jnp.einsum(
        "spd,dc->spc", tok_rows, key_projection_weight, preferred_element_type=jnp.float32
    )
    split_heads = key_raw.reshape(key_raw.shape[:2] + (-1, head_dim))
    normed = (
        split_heads
        * lax.rsqrt(jnp.mean(split_heads * split_heads, axis=-1, keepdims=True) + EPSILON)
        * key_norm_gain
    )
    block_keys = normed.astype(jnp.bfloat16)
    block_values = jnp.einsum(
        "spd,dc->spc", tok_rows, value_projection_weight, preferred_element_type=jnp.float32
    )
    block_values = block_values.reshape(split_heads.shape).astype(jnp.bfloat16)
    cache_rows = jnp.concatenate([block_keys, block_values], axis=-1)
    gate_preactivation = jnp.einsum(
        "spd,hd->shp", tok_rows, forget_gate_weight, preferred_element_type=jnp.float32
    )
    return (cache_rows, gate_preactivation + forget_gate_bias[None, :, None])


def forget_value_rows(gate_preactivation, forget_gate_scale, gate_spike_added):
    return forget_gate_scale * jax.nn.log_sigmoid(gate_preactivation) + gate_spike_added


def query_split(query, kv_count, head_dim):
    return query.reshape(query.shape[0], kv_count, -1, head_dim)


def head_scores(query, cache_rows, head_dim):
    query_heads = query_split(query, cache_rows.shape[2], head_dim)
    key_heads = cache_rows[..., :head_dim]
    return jnp.einsum(
        "skge,slke->skgl", query_heads, key_heads, preferred_element_type=jnp.float32
    ) * head_dim ** (-0.5)


def weigh(scores, cache_rows, head_dim):
    row_top = jnp.max(scores, axis=-1)
    weights = jnp.exp(scores - row_top[..., None]).astype(jnp.bfloat16)
    value_heads = cache_rows[..., head_dim:]
    return (
        row_top,
        jnp.einsum("skgl,slke->skge", weights, value_heads, preferred_element_type=jnp.float32),
    )


def local(
    prompt_block_input,
    key_projection_weight,
    value_projection_weight,
    forget_gate_weight,
    forget_gate_bias,
    forget_gate_scale,
    gate_spike_added,
    prior_key_value_cache,
    prior_cumulative_log_forget,
    decoded_token_query,
    decoded_token_key,
    decoded_token_value,
    decoded_log_gate,
    key_norm_gain,
    read_norm_gain,
):
    head_dim = key_norm_gain.shape[0]
    own_count = prior_key_value_cache.shape[0]
    kv_count = prior_key_value_cache.shape[2]
    seq_start = lax.axis_index("sp") * own_count
    query_own = lax.dynamic_slice_in_dim(decoded_token_query, seq_start, own_count, 0)
    rows_local, gate_preactivation = project(
        prompt_block_input,
        key_projection_weight,
        value_projection_weight,
        forget_gate_weight,
        forget_gate_bias,
        key_norm_gain,
    )
    local_forget_values = forget_value_rows(gate_preactivation, forget_gate_scale, gate_spike_added)
    new_cache = lax.all_to_all(rows_local, "sp", split_axis=0, concat_axis=1, tiled=True)
    log_forget_value = lax.all_to_all(
        local_forget_values, "sp", split_axis=0, concat_axis=2, tiled=True
    )
    new_logc = prior_cumulative_log_forget[:, :, -1:] + jnp.cumsum(log_forget_value, axis=-1)
    final_logc = new_logc[:, :, -1] + decoded_log_gate
    past_scores = (
        head_scores(query_own, prior_key_value_cache, head_dim)
        + final_logc[:, :, None, None]
        - prior_cumulative_log_forget[:, :, None, :]
    )
    past_top, past_sum = weigh(past_scores, prior_key_value_cache, head_dim)
    block_scores = (
        head_scores(query_own, new_cache, head_dim)
        + final_logc[:, :, None, None]
        - new_logc[:, :, None, :]
    )
    block_top, block_sum = weigh(block_scores, new_cache, head_dim)
    query_heads = query_split(query_own, kv_count, head_dim)
    own_keys = decoded_token_key.reshape(own_count, kv_count, head_dim)
    own_score = jnp.einsum(
        "skge,ske->skg", query_heads, own_keys, preferred_element_type=jnp.float32
    ) * head_dim ** (-0.5)
    row_top = jnp.maximum(jnp.maximum(past_top, block_top), own_score)
    own_weight = jnp.exp(own_score - row_top).astype(jnp.bfloat16)
    weighted = (
        past_sum * jnp.exp(past_top - row_top)[..., None]
        + block_sum * jnp.exp(block_top - row_top)[..., None]
    )
    own_values = decoded_token_value.reshape(own_count, kv_count, 1, head_dim).astype(jnp.float32)
    weighted = weighted + own_weight.astype(jnp.float32)[..., None] * own_values
    normed = weighted * lax.rsqrt(jnp.mean(weighted * weighted, axis=-1, keepdims=True) + EPSILON)
    next_read = (normed.reshape(own_count, -1) * read_norm_gain).astype(jnp.bfloat16)
    return (new_cache, new_logc, next_read)


def solution(mesh):
    return jax.shard_map(
        local,
        mesh=mesh,
        in_specs=(
            P("gr", "sp", None),
            P(None, "tp"),
            P(None, "tp"),
            P("tp", None),
            P("tp"),
            P("gr", "tp", "sp"),
            P("gr", "tp", "sp"),
            P(("gr", "sp"), None, "tp", None),
            P(("gr", "sp"), "tp", None),
            P("gr", "tp"),
            P(("gr", "sp"), "tp"),
            P(("gr", "sp"), "tp"),
            P(("gr", "sp"), "tp"),
            P(),
            P("tp"),
        ),
        out_specs=(
            P(("gr", "sp"), None, "tp", None),
            P(("gr", "sp"), "tp", None),
            P(("gr", "sp"), "tp"),
        ),
        check_vma=False,
    )
```

profile of v0, /device:TPU:0, one launch (start us, length us, event | category | flops | bytes accessed | tf_op | source)
XLA Modules:
  0.0 118.0 jit_solution(34637716511074179)
XLA Ops:
  0.6 0.0 copy-start
  0.6 6.4 %fusion.20 = f32[8,4,256]{2,1,0:T(4,128)} fusion(f32[8,4,256]{2,1,0:T(4,128)} %param.21, f32[8,4,256]{2,1,0:T(4,128)} %param.20, bf16[8,256,2048]{2,1,0:T(8,128)(2,1)} %param.15, bf16[4,2048]{1,0:T(4,128)(2,1)} %param.18, f32[4]{0:T(128)} %param.19), kind=kOutput, calls=%fused_computation.31 | convolution fusion | flops 33644544 | bytes 8503312 | tf_op jit(solution)/shard_map/spd,hd->shp/dot_general | solution.py:33
  7.0 7.3 %all-to-all-start.1 = ((f32[8,4,256]{2,1,0:T(4,128)}), f32[8,4,256]{2,1,0:T(4,128)S(1)}, u32[]{:S(2)}, u32[]{:S(2)}) async-start(f32[8,4,256]{2,1,0:T(4,128)} %fusion.20), calls=%async_computation.1 | async-start | bytes 65536 | tf_op jit(solution)/shard_map/all_to_all | solution.py:97
  14.3 0.0 copy-done
  14.3 0.0 copy-start.2
  14.4 0.0 copy-start.9
  14.4 5.9 %multiply_reduce_fusion = (f32[8,256,4]{1,2,0:T(4,128)S(1)}, f32[8,256,256]{1,2,0:T(8,128)S(1)}) fusion(bf16[8,256,2048]{2,1,0:T(8,128)(2,1)} %param.15, bf16[2048,256]{1,0:T(8,128)(2,1)S(1)} %copy-done), kind=kOutput, calls=%fused_computation.11 | convolution fusion | flops 2148524032 | bytes 11567104 | tf_op jit(solution)/shard_map/spd,dc->spc/dot_general | solution.py:18
  20.3 0.0 copy-done.2
  20.3 0.0 copy-done.9
  20.4 0.0 copy-start.8
  20.4 2.4 %convolution_convert_fusion = bf16[8,256,256]{1,2,0:T(8,128)(2,1)S(1)} fusion(bf16[8,256,2048]{2,1,0:T(8,128)(2,1)S(1)} %copy-done.2, bf16[2048,256]{1,0:T(8,128)(2,1)S(1)} %copy-done.9), kind=kOutput, calls=%fused_computation.12 | convolution fusion | flops 2148007936 | bytes 10485760 | tf_op jit(solution)/shard_map/spd,dc->spc/dot_general | solution.py:28
  22.8 0.0 copy-done.8
  22.8 0.6 multiply_convert_fusion
  23.4 1.5 %pad_maximum_fusion = bf16[8,256,4,128]{1,3,2,0:T(8,128)(2,1)} fusion(bf16[8,256,4,64]{1,3,2,0:T(8,128)(2,1)S(1)} %bitcast.80, bf16[8,256,4,64]{1,3,2,0:T(8,128)(2,1)S(1)} %multiply_convert_fusion), kind=kLoop, calls=%fused_computation.9 | loop fusion | flops 4194304 | bytes 4194304 | tf_op jit(solution)/shard_map/concatenate | solution.py:32
  24.8 0.0 all-to-all-done.1
  24.9 6.0 %all-to-all-start = ((bf16[8,256,4,128]{1,3,2,0:T(8,128)(2,1)}), bf16[8,256,4,128]{1,3,2,0:T(8,128)(2,1)S(1)}, u32[]{:S(2)}, u32[]{:S(2)}) async-start(bf16[8,256,4,128]{1,3,2,0:T(8,128)(2,1)} %pad_maximum_fusion), calls=%async_computation | async-start | bytes 4194304 | tf_op jit(solution)/shard_map/all_to_all | solution.py:96
  30.8 20.9 %fusion.26 = (bf16[1,14336,4,64]{3,2,1,0:T(4,128)(2,1)}, bf16[1,14336,4,64]{3,2,1,0:T(4,128)(2,1)}) fusion(bf16[1,14336,4,128]{3,2,1,0:T(4,128)(2,1)} %param.22), kind=kLoop, calls=%fused_computation.56 | loop fusion | bytes 29360128 | tf_op jit(solution)/shard_map/slice | solution.py:49
  51.8 0.7 dynamic-slice_reduce_fusion
  52.5 0.1 reshape.260
  52.6 21.4 %copy.37 = bf16[1,14336,4,64]{1,3,2,0:T(8,128)(2,1)} copy(bf16[1,14336,4,64]{3,2,1,0:T(4,128)(2,1)} %get-tuple-element.9) | data formatting | bytes 14680064
  74.0 0.0 copy-done.6
  74.1 0.1 reshape.276
  74.1 21.4 %copy.38 = bf16[1,14336,4,64]{1,3,2,0:T(8,128)(2,1)} copy(bf16[1,14336,4,64]{3,2,1,0:T(4,128)(2,1)} %get-tuple-element.10) | data formatting | bytes 14680064
  95.6 0.1 reshape.269
  95.7 0.2 slice_reduce_fusion.2
  95.9 0.1 fusion.29
  96.0 1.2 reduce-window.6
  97.2 0.2 slice_reduce_fusion
  97.4 0.2 reduce-window.9
  97.6 0.1 broadcast.92
  97.7 0.1 add_add_fusion
  97.7 0.2 slice_reduce_fusion.1
  97.9 0.0 copy-done.10
  97.9 0.1 broadcast_bitcast_fusion
  98.0 0.1 fusion.21
  98.1 4.9 %fusion.27 = (f32[4,2]{1,0:T(4,128)S(1)}, f32[4,2,14336]{2,1,0:T(2,128)}) fusion(f32[4,14336]{1,0:T(4,128)S(1)} %bitcast.79, f32[4]{0:T(128)S(1)} %fusion.25, bf16[4,2,64]{2,1,0:T(2,128)(2,1)S(1)} %reshape.260, bf16[1,14336,4,64]{1,3,2,0:T(8,128)(2,1)} %copy.37), kind=kOutput, calls=%fused_computation.57 | convolution fusion | flops 15138808 | bytes 8029232 | tf_op jit(solution)/shard_map/skge,slke->skgl/dot_general | solution.py:50
  103.0 0.0 all-to-all-done
  103.0 2.5 %copy.26 = bf16[8,256,4,128]{1,0,3,2:T(8,128)(2,1)} copy(bf16[8,256,4,128]{1,3,2,0:T(8,128)(2,1)S(1)} %all-to-all-done) | data formatting | bytes 4194304 | tf_op jit(solution)/shard_map/all_to_all | solution.py:96
  105.5 3.0 %all_to_all.21 = bf16[1,2048,4,128]{1,3,2,0:T(8,128)(2,1)S(1)} reshape(bf16[8,256,4,128]{1,0,3,2:T(8,128)(2,1)} %copy.26) | data formatting | bytes 4194304 | tf_op jit(solution)/shard_map/all_to_all | solution.py:96
  108.5 0.0 copy-start.5
  108.5 2.5 %copy.30 = bf16[1,2048,4,128]{3,2,1,0:T(4,128)(2,1)} copy(bf16[1,2048,4,128]{1,3,2,0:T(8,128)(2,1)S(1)} %all_to_all.21) | data formatting | bytes 4194304
  111.1 0.3 fusion.28
  111.4 5.3 %fusion.11 = f32[4,2,64]{2,1,0:T(2,128)S(1)} fusion(bf16[1,14336,4,64]{1,3,2,0:T(8,128)(2,1)} %copy.38, f32[4,2,14336]{2,1,0:T(2,128)} %get-tuple-element.17, f32[4,2]{1,0:T(4,128)S(1)} %get-tuple-element.16, f32[4,2]{1,0:T(4,128)S(1)} %get-tuple-element.13), kind=kOutput, calls=%fused_computation.19 | convolution fusion | flops 14909952 | bytes 7800896 | tf_op jit(solution)/shard_map/skgl,slke->skge/dot_general | solution.py:61
  116.7 0.5 multiply_reduce_fusion.1
  117.3 0.1 broadcast_multiply_fusion
  117.3 0.1 reshape.268
  117.4 0.0 copy-done.5
  117.4 0.6 convert_element_type.52
  (22 shorter events, 0.2 us)
Async XLA Ops:
  0.6 13.7 %copy-start = (bf16[2048,256]{1,0:T(8,128)(2,1)S(1)}, bf16[2048,256]{1,0:T(8,128)(2,1)}, u32[]{:S(2)}) copy-start(bf16[2048,256]{1,0:T(8,128)(2,1)} %param.16) | copy-start | bytes 3145732
  7.0 17.8 %all-to-all-start.1 = ((f32[8,4,256]{2,1,0:T(4,128)}), f32[8,4,256]{2,1,0:T(4,128)S(1)}, u32[]{:S(2)}, u32[]{:S(2)}) async-start(f32[8,4,256]{2,1,0:T(4,128)} %fusion.20), calls=%async_computation.1 | async-start | bytes 65536 | tf_op jit(solution)/shard_map/all_to_all | solution.py:97
  14.3 6.0 %copy-start.2 = (bf16[8,256,2048]{2,1,0:T(8,128)(2,1)S(1)}, bf16[8,256,2048]{2,1,0:T(8,128)(2,1)}, u32[]{:S(2)}) copy-start(bf16[8,256,2048]{2,1,0:T(8,128)(2,1)} %param.15) | copy-start | bytes 25165828
  14.4 6.0 %copy-start.9 = (bf16[2048,256]{1,0:T(8,128)(2,1)S(1)}, bf16[2048,256]{1,0:T(8,128)(2,1)}, u32[]{:S(2)}) copy-start(bf16[2048,256]{1,0:T(8,128)(2,1)} %param.17) | copy-start | bytes 3145732
  20.4 2.4 %copy-start.8 = (f32[64]{0:T(128)S(1)}, f32[64]{0:T(128)}, u32[]{:S(2)}) copy-start(f32[64]{0:T(128)} %param.28) | copy-start | bytes 772
  24.9 78.2 %all-to-all-start = ((bf16[8,256,4,128]{1,3,2,0:T(8,128)(2,1)}), bf16[8,256,4,128]{1,3,2,0:T(8,128)(2,1)S(1)}, u32[]{:S(2)}, u32[]{:S(2)}) async-start(bf16[8,256,4,128]{1,3,2,0:T(8,128)(2,1)} %pad_maximum_fusion), calls=%async_computation | async-start | bytes 4194304 | tf_op jit(solution)/shard_map/all_to_all | solution.py:96
  52.6 21.4 %copy-start.6 = (bf16[1,256]{1,0:T(2,128)(2,1)S(1)}, bf16[1,256]{1,0:T(2,128)(2,1)}, u32[]{:S(2)}) copy-start(bf16[1,256]{1,0:T(2,128)(2,1)} %param.25) | copy-start | bytes 1540
  74.1 21.5 %copy-start.7 = (bf16[1,256]{1,0:T(2,128)(2,1)S(1)}, bf16[1,256]{1,0:T(2,128)(2,1)}, u32[]{:S(2)}) copy-start(bf16[1,256]{1,0:T(2,128)(2,1)} %param.26) | copy-start | bytes 1540
  74.1 21.6 %copy-start.3 = (f32[1,4,14336]{2,1,0:T(4,128)S(1)}, f32[1,4,14336]{2,1,0:T(4,128)}, u32[]{:S(2)}) copy-start(f32[1,4,14336]{2,1,0:T(4,128)} %param.23) | copy-start | bytes 688132
  74.1 23.8 %copy-start.10 = (f32[1,4]{1,0:T(1,128)S(1)}, f32[1,4]{1,0:T(1,128)}, u32[]{:S(2)}) copy-start(f32[1,4]{1,0:T(1,128)} %param.27) | copy-start | bytes 52
  97.7 10.8 %copy-start.4 = (f32[1,4,2048]{2,1,0:T(4,128)}, f32[1,4,2048]{2,1,0:T(4,128)S(1)}, u32[]{:S(2)}) copy-start(f32[1,4,2048]{2,1,0:T(4,128)S(1)} %add_add_fusion) | copy-start | bytes 98308
  105.5 12.5 %copy-start.1 = (bf16[2048,256]{1,0:T(8,128)(2,1)S(1)}, bf16[2048,256]{1,0:T(8,128)(2,1)}, u32[]{:S(2)}) copy-start(bf16[2048,256]{1,0:T(8,128)(2,1)} %param.16) | copy-start | bytes 3145732
  108.5 8.9 %copy-start.5 = (f32[512]{0:T(512)S(1)}, f32[512]{0:T(512)}, u32[]{:S(2)}) copy-start(f32[512]{0:T(512)} %param.29) | copy-start | bytes 6148
where the time goes:
time: 119 us; the launch traced here: 118 us
  local copies, waits for them, and re-layouts  74.3 us (62%)
  matrix products  25.9 us (22%)
  starting transfers between devices  13.3 us (11%)
  other arithmetic  3.72 us (3%)
    unnamed x26, local copies, waits for them, and re-layouts  45.6 us
    slice x1, local copies, waits for them, and re-layouts, head_scores(): key_heads = cache_rows[..., :head_dim]  20.9 us
    all_to_all x1, starting transfers between devices, local(): lax.all_to_all(local_forget_values, 'sp', split_axis=0, concat_axis=2, ti...  7.31 us
    dot_general x1, matrix products, project(): jnp.einsum('spd,hd->shp', tok_rows, forget_gate_weight, preferred_element...  6.38 us
    all_to_all x1, starting transfers between devices, local(): lax.all_to_all(rows_local, 'sp', split_axis=0, concat_axis=1, tiled=True)  5.99 us
    dot_general x1, matrix products, project(): jnp.einsum('spd,dc->spc', tok_rows, key_projection_weight, preferred_elem...  5.92 us
    dot_general x2, matrix products, weigh(): jnp.einsum('skgl,slke->skge', weights, value_heads, preferred_element_typ...  5.84 us
    all_to_all x2, local copies, waits for them, and re-layouts, local(): lax.all_to_all(rows_local, 'sp', split_axis=0, concat_axis=1, tiled=True)  5.47 us
  transfers between devices with their start and end apart: 2, of which 0 were waited for; matrix products, arithmetic and copies ran while one was open for 70% of the time, Pallas kernels for 0%

commit v1 on v0

v1 whole, which is shorter than its diff:
```python
import functools

import jax
import jax.numpy as jnp
from jax import lax
from jax.experimental import pallas as pl
from jax.experimental.pallas import tpu as pltpu
from jax.sharding import PartitionSpec as P

EPSILON = 1e-06
LOW = -1e30
MESH = pl.DeviceIdType.MESH
F32 = jnp.float32
BF16 = jnp.bfloat16


def step_pair(i, n):
    m = max(n // 2, 1)
    return 2 * ((m // 2 + m - i // 2) % m) + i % 2


def flip(me, k, n):
    if n & (n - 1):
        return (me + k) % n
    out = 0
    bit = 1
    while bit < n:
        a = (me // bit) % 2
        b = (k // bit) % 2
        out = out + bit * (a + b - 2 * a * b)
        bit *= 2
    return out


def back(me, k, n):
    if n & (n - 1):
        return (me + n - k) % n
    return flip(me, k, n)


def expander(positions, kv):
    shape = (positions, positions * kv)
    p = lax.broadcasted_iota(jnp.int32, shape, 0)
    r = lax.broadcasted_iota(jnp.int32, shape, 1)
    return jnp.where((r >= p * kv) & (r < p * kv + kv), 1.0, 0.0).astype(BF16)


def expand(values, matrix):
    rows = values.shape[0]
    high = values.astype(BF16).astype(F32)
    rest = values - high
    middle = rest.astype(BF16).astype(F32)
    low = rest - middle
    pieces = jnp.concatenate([high, middle, low], axis=0).astype(BF16)
    out = jnp.dot(pieces, matrix, preferred_element_type=F32)
    return out[:rows] + out[rows : 2 * rows] + out[2 * rows :]


def column(row):
    k = row.shape[1]
    eye = lax.broadcasted_iota(jnp.int32, (k, k), 0) == lax.broadcasted_iota(jnp.int32, (k, k), 1)
    return jnp.sum(jnp.where(eye, jnp.broadcast_to(row, (k, k)), 0.0), axis=1, keepdims=True)


def same_head(rows, count, kv):
    a = lax.broadcasted_iota(jnp.int32, (rows, count), 0)
    b = lax.broadcasted_iota(jnp.int32, (rows, count), 1)
    return lax.rem(a, kv) == lax.rem(b, kv)


def attend(query, keys, bias, scale, kv):
    s = lax.dot_general(query, keys, (((1,), (1,)), ((), ())), preferred_element_type=F32)
    s = s * scale + bias
    return jnp.where(same_head(s.shape[0], s.shape[1], kv), s, LOW)


def kernel(
    dims,
    x_hbm, wk_hbm, wv_hbm, wg_ref, bias_ref, scale_ref, spike_ref, cache_hbm, prior_hbm,
    query_ref, own_key_ref, own_value_ref, own_gate_ref, key_gain_ref, read_gain_ref,
    new_cache_hbm, new_logc_ref, read_ref,
    x_v, wk_v, wv_v, cache_v, prior_v, stage, send_v, recv_v, csend_v, crecv_v,
    expand_v, part_m, part_acc,
    x_sem, w_sem, cache_sem, prior_sem, send_sem, recv_sem, csend_sem, crecv_sem, out_sem,
):
    n, span, kv, head_dim, group, reps, chunk, sub = dims
    rows = reps * kv
    chunks = cache_sem.shape[0]
    chunk_rows = chunk * kv
    att_scale = head_dim ** (-0.5)
    me = lax.axis_index("sp")

    def x_copy(i):
        s = flip(me, step_pair(i, n), n)
        return pltpu.make_async_copy(x_hbm.at[s], x_v.at[s], x_sem.at[i])

    def cache_copy(c):
        at = pl.ds(pl.multiple_of(c * chunk_rows, chunk_rows), chunk_rows)
        return pltpu.make_async_copy(cache_hbm.at[at], cache_v.at[at], cache_sem.at[c])

    wk_copy = pltpu.make_async_copy(wk_hbm, wk_v, w_sem.at[0])
    wv_copy = pltpu.make_async_copy(wv_hbm, wv_v, w_sem.at[1])
    prior_copy = pltpu.make_async_copy(prior_hbm, prior_v, prior_sem)
    x_copy(0).start()
    wk_copy.start()
    wv_copy.start()

    @pl.loop(1, n)
    def _(i):
        x_copy(i).start()

    barrier = pltpu.get_barrier_semaphore()

    @pl.loop(1, n)
    def _(k):
        pl.semaphore_signal(barrier, inc=1, device_id={"sp": (me + k) % n}, device_id_type=MESH)

    prior_copy.start()

    @pl.loop(0, chunks)
    def _(c):
        cache_copy(c).start()

    expand_v[...] = expander(sub, kv)
    bias_col = column(bias_ref[...])
    own_gate_col = column(own_gate_ref[...])
    key_gain = key_gain_ref[...]
    upper = jnp.where(
        lax.broadcasted_iota(jnp.int32, (span, span), 0) <= lax.broadcasted_iota(jnp.int32, (span, span), 1),
        1.0, 0.0,
    )
    pl.semaphore_wait(barrier, n - 1)
    wk_copy.wait()
    wv_copy.wait()

    def remote(i, s):
        return (
            pltpu.make_async_remote_copy(
                src_ref=send_v.at[i], dst_ref=recv_v.at[me], send_sem=send_sem.at[i],
                recv_sem=recv_sem.at[me], device_id={"sp": s}, device_id_type=MESH,
            ),
            pltpu.make_async_remote_copy(
                src_ref=csend_v.at[i], dst_ref=crecv_v.at[me], send_sem=csend_sem.at[i],
                recv_sem=crecv_sem.at[me], device_id={"sp": s}, device_id_type=MESH,
            ),
        )

    @pl.loop(0, n)
    def _(i):
        k = step_pair(i, n)
        s = flip(me, k, n)
        x_copy(i).wait()
        xb = x_v[s]
        keys = jnp.dot(xb, wk_v[...], preferred_element_type=F32)
        values = jnp.dot(xb, wv_v[...], preferred_element_type=F32)
        for h in range(kv):
            kh = keys[:, h * head_dim : (h + 1) * head_dim]
            vh = values[:, h * head_dim : (h + 1) * head_dim]
            kh = kh * lax.rsqrt(jnp.mean(kh * kh, axis=-1, keepdims=True) + EPSILON) * key_gain
            row = jnp.concatenate([kh, vh], axis=-1)
            if kv == 1:
                stage[...] = row
            else:
                stage[pl.ds(h, span, stride=kv), :] = row
        send_v[i] = stage[...].astype(BF16)
        pre = lax.dot_general(
            wg_ref[...], xb, (((1,), (1,)), ((), ())), preferred_element_type=F32
        ) + bias_col
        log_sig = jnp.minimum(pre, 0.0) - jnp.log1p(jnp.exp(-jnp.abs(pre)))
        log_forget = scale_ref[s] * log_sig + spike_ref[s]
        csend_v[i] = jnp.dot(
            log_forget, upper, preferred_element_type=F32, precision=lax.Precision.HIGHEST
        )

        @pl.when(k != 0)
        def _():
            block, sums = remote(i, s)
            sums.start()
            block.start()

        @pl.when(k == 0)
        def _():
            pltpu.make_async_copy(send_v.at[i], recv_v.at[me], recv_sem.at[me]).start()
            pltpu.make_async_copy(csend_v.at[i], crecv_v.at[me], crecv_sem.at[me]).start()

    every = query_ref[...].astype(F32)
    own = lax.broadcasted_iota(jnp.int32, every.shape, 0) == me
    all_query = jnp.sum(jnp.where(own, every, 0.0), axis=0, keepdims=True)
    zeros = jnp.zeros((1, head_dim), F32)
    pieces = []
    for rep in range(reps):
        for h in range(kv):
            at = (h * group + rep % group) * head_dim
            pieces.append(jnp.concatenate([all_query[:, at : at + head_dim], zeros], axis=1))
    query = jnp.concatenate(pieces, axis=0)
    query_b = query.astype(BF16)

    prior_copy.wait()
    prior_last = prior_v[:, prior_v.shape[1] - 1 :]

    def repeat_rows(values):
        return jnp.concatenate([values] * reps, axis=0)

    def past_step(c, carry):
        top, acc = carry
        cache_copy(c).wait()
        keys = cache_v[pl.ds(pl.multiple_of(c * chunk_rows, chunk_rows), chunk_rows), :]
        distance = repeat_rows(prior_last - prior_v[:, pl.ds(pl.multiple_of(c * chunk, chunk), chunk)])
        bias = jnp.concatenate(
            [expand(distance[:, j * sub : (j + 1) * sub], expand_v[...]) for j in range(chunk // sub)], axis=1
        )
        s = attend(query_b, keys, bias, att_scale, kv)
        new_top = jnp.maximum(top, jnp.max(s, axis=1, keepdims=True))
        weights = jnp.exp(s - new_top).astype(BF16)
        acc = acc * jnp.exp(top - new_top) + jnp.dot(weights, keys, preferred_element_type=F32)
        return new_top, acc

    past_top, past_acc = lax.fori_loop(
        0, chunks, past_step,
        (jnp.full((rows, 1), LOW, F32), jnp.zeros((rows, 2 * head_dim), F32)),
    )

    block_expander = expander(span, kv)

    def out_copy(b):
        at = pl.ds(pl.multiple_of(b * span * kv, span * kv), span * kv)
        return pltpu.make_async_copy(recv_v.at[b], new_cache_hbm.at[at], out_sem.at[b])

    @pl.loop(0, n)
    def _(i):
        k = step_pair(i, n)
        b = back(me, k, n)

        @pl.when(k != 0)
        def _():
            pltpu.make_async_remote_copy(
                src_ref=csend_v.at[i], dst_ref=crecv_v.at[b], send_sem=csend_sem.at[i],
                recv_sem=crecv_sem.at[b], device_id={"sp": b}, device_id_type=MESH,
            ).wait_recv()
            pltpu.make_async_remote_copy(
                src_ref=send_v.at[i], dst_ref=recv_v.at[b], send_sem=send_sem.at[i],
                recv_sem=recv_sem.at[b], device_id={"sp": b}, device_id_type=MESH,
            ).wait_recv()

        @pl.when(k == 0)
        def _():
            pltpu.make_async_copy(csend_v.at[i], crecv_v.at[b], crecv_sem.at[b]).wait()
            pltpu.make_async_copy(send_v.at[i], recv_v.at[b], recv_sem.at[b]).wait()

        out_copy(b).start()
        keys = recv_v[b]
        bias = expand(repeat_rows(-crecv_v[b]), block_expander)
        s = attend(query_b, keys, bias, att_scale, kv)
        top = jnp.max(s, axis=1, keepdims=True)
        weights = jnp.exp(s - top).astype(BF16)
        part_m[b] = jnp.broadcast_to(top, (rows, 2 * head_dim))
        part_acc[b] = jnp.dot(weights, keys, preferred_element_type=F32)

    before = jnp.zeros((kv, 1), F32)
    tops = [past_top]
    accs = [past_acc]
    for b in range(n):
        sums = crecv_v[b]
        new_logc_ref[:, b * span : (b + 1) * span] = prior_last + before + sums
        tops.append(part_m[b][:, :1] - repeat_rows(before))
        accs.append(part_acc[b])
        before = before + sums[:, span - 1 :]
    final = repeat_rows(before + own_gate_col)

    own_key = own_key_ref[...].astype(F32)
    own_value = own_value_ref[...].astype(F32)
    own_keys = jnp.concatenate(
        [own_key[:, h * head_dim : (h + 1) * head_dim] for _ in range(reps) for h in range(kv)], axis=0
    )
    own_values = jnp.concatenate(
        [own_value[:, h * head_dim : (h + 1) * head_dim] for _ in range(reps) for h in range(kv)], axis=0
    )
    own_top = jnp.sum(query[:, :head_dim] * own_keys, axis=1, keepdims=True) * att_scale - final
    row_top = own_top
    for t in tops:
        row_top = jnp.maximum(row_top, t)
    total = jnp.zeros((rows, 2 * head_dim), F32)
    for t, a in zip(tops, accs):
        total = total + a * jnp.exp(t - row_top)
    own_weight = jnp.exp(own_top - row_top).astype(BF16).astype(F32)
    weighted = total[:, head_dim:] + own_weight * own_values
    normed = weighted * lax.rsqrt(jnp.mean(weighted * weighted, axis=1, keepdims=True) + EPSILON)
    flat = jnp.concatenate(
        [normed[g * kv + h : g * kv + h + 1, :] for h in range(kv) for g in range(group)], axis=1
    )
    read_ref[...] = (flat * read_gain_ref[...]).astype(BF16)

    @pl.loop(0, n)
    def _(i):
        k = step_pair(i, n)
        s = flip(me, k, n)
        out_copy(s).wait()

        @pl.when(k != 0)
        def _():
            block, sums = remote(i, s)
            sums.wait_send()
            block.wait_send()


def local(
    n,
    prompt_block_input,
    key_projection_weight,
    value_projection_weight,
    forget_gate_weight,
    forget_gate_bias,
    forget_gate_scale,
    gate_spike_added,
    prior_key_value_cache,
    prior_cumulative_log_forget,
    decoded_token_query,
    decoded_token_key,
    decoded_token_value,
    decoded_log_gate,
    key_norm_gain,
    read_norm_gain,
):
    head_dim = key_norm_gain.shape[0]
    _, past, kv, width = prior_key_value_cache.shape
    _, span, model = prompt_block_input.shape
    group = decoded_token_query.shape[1] // (kv * head_dim)
    reps = max(group, -(-8 // kv))
    rows = reps * kv
    sub = 256
    chunk = 1024
    while past % chunk:
        chunk //= 2
    sub = min(sub, chunk)
    chunks = past // chunk
    block_rows = span * kv
    vmem = pl.BlockSpec(memory_space=pltpu.VMEM)
    hbm = pl.BlockSpec(memory_space=pl.ANY)
    new_cache, new_logc, read = pl.pallas_call(
        functools.partial(kernel, (n, span, kv, head_dim, group, reps, chunk, sub)),
        out_shape=(
            jax.ShapeDtypeStruct((n * block_rows, width), BF16),
            jax.ShapeDtypeStruct((kv, n * span), F32),
            jax.ShapeDtypeStruct((1, group * kv * head_dim), BF16),
        ),
        in_specs=[hbm, hbm, hbm, vmem, vmem, vmem, vmem, hbm, hbm] + [vmem] * 6,
        out_specs=(hbm, vmem, vmem),
        scratch_shapes=[
            pltpu.VMEM((n, span, model), BF16),
            pltpu.VMEM((model, kv * head_dim), BF16),
            pltpu.VMEM((model, kv * head_dim), BF16),
            pltpu.VMEM((past * kv, width), BF16),
            pltpu.VMEM((kv, past), F32),
            pltpu.VMEM((block_rows, width), F32),
            pltpu.VMEM((n, block_rows, width), BF16),
            pltpu.VMEM((n, block_rows, width), BF16),
            pltpu.VMEM((n, kv, span), F32),
            pltpu.VMEM((n, kv, span), F32),
            pltpu.VMEM((sub, sub * kv), BF16),
            pltpu.VMEM((n, rows, width), F32),
            pltpu.VMEM((n, rows, width), F32),
            pltpu.SemaphoreType.DMA((n,)),
            pltpu.SemaphoreType.DMA((2,)),
            pltpu.SemaphoreType.DMA((chunks,)),
            pltpu.SemaphoreType.DMA,
            pltpu.SemaphoreType.DMA((n,)),
            pltpu.SemaphoreType.DMA((n,)),
            pltpu.SemaphoreType.DMA((n,)),
            pltpu.SemaphoreType.DMA((n,)),
            pltpu.SemaphoreType.DMA((n,)),
        ],
        compiler_params=pltpu.CompilerParams(
            collective_id=0, has_side_effects=True, vmem_limit_bytes=60 * 1024 * 1024
        ),
    )(
        prompt_block_input,
        key_projection_weight,
        value_projection_weight,
        forget_gate_weight,
        forget_gate_bias.reshape(1, -1),
        forget_gate_scale,
        gate_spike_added,
        prior_key_value_cache.reshape(past * kv, width),
        prior_cumulative_log_forget.reshape(kv, past),
        decoded_token_query,
        decoded_token_key,
        decoded_token_value,
        decoded_log_gate,
        key_norm_gain.reshape(1, -1),
        read_norm_gain.reshape(1, -1),
    )
    return (
        new_cache.reshape(1, n * span, kv, width),
        new_logc.reshape(1, kv, n * span),
        read,
    )


def solution(mesh):
    return jax.shard_map(
        functools.partial(local, mesh.shape["sp"]),
        mesh=mesh,
        in_specs=(
            P("gr", "sp", None),
            P(None, "tp"),
            P(None, "tp"),
            P("tp", None),
            P("tp"),
            P("gr", "tp", "sp"),
            P("gr", "tp", "sp"),
            P(("gr", "sp"), None, "tp", None),
            P(("gr", "sp"), "tp", None),
            P("gr", "tp"),
            P(("gr", "sp"), "tp"),
            P(("gr", "sp"), "tp"),
            P(("gr", "sp"), "tp"),
            P(),
            P("tp"),
        ),
        out_specs=(
            P(("gr", "sp"), None, "tp", None),
            P(("gr", "sp"), "tp", None),
            P(("gr", "sp"), "tp"),
        ),
        check_vma=False,
    )
```

time: 119 us -> 62.3 us (0.52)
  the two profiles are of different devices: /device:TPU:0 before, /device:TPU:8 now
where the time goes in v1:
time: 62.3 us; the launch traced here: 62 us
  Pallas kernels  55.8 us (90%)
  local copies, waits for them, and re-layouts  5.56 us (9%)
  between operations  0.65 us (1%)
    pallas_call x1, Pallas kernels, local(): pl.pallas_call(functools.partial(kernel, (n, span, kv, head_dim, group, r...  55.8 us
    unnamed x3, local copies, waits for them, and re-layouts  5.56 us

profile of v1, /device:TPU:8, one launch (start us, length us, event | category | flops | bytes accessed | tf_op | source)
XLA Modules:
  0.0 62.0 jit_solution(3446611037964256485)
XLA Ops:
  0.6 55.8 %shard_map.166 = (bf16[8192,128]{1,0:T(8,128)(2,1)}, f32[4,2048]{1,0:T(4,128)}, bf16[1,512]{1,0:T(2,128)(2,1)}) custom-call(bf16[8,256,2048]{2,1,0:T(8,128)(2,1)} %x_hbm.1, bf16[2048,256]{1,0:T(8,128)(2,1)} %wk_hbm.1, bf16[2048,256]{1,0:T(8,128)(2,1)} %wv_hbm.1, bf16[4,2048]{1,0:T(4,128)(2,1)} %wg_ref.1, f32[1,4]{1,0:T(1,128)} %bitcast.12, ...), custom_call_target="tpu_custom_call" | custom-call | tf_op jit(solution)/shard_map/pallas_call | solution.py:339
  56.5 2.9 %copy.21 = bf16[1,2048,4,128]{3,2,1,0:T(4,128)(2,1)} copy(bf16[1,2048,4,128]{3,2,1,0:T(4,128)(2,1)} %bitcast.8) | data formatting | bytes 4194304
  59.4 1.4 %copy.22 = f32[1,4,2048]{2,1,0:T(4,128)} copy(f32[1,4,2048]{2,1,0:T(4,128)} %bitcast.10) | data formatting | bytes 65536
  60.8 1.3 %copy.23 = bf16[1,512]{1,0:T(2,128)(2,1)} copy(bf16[1,512]{1,0:T(2,128)(2,1)} %get-tuple-element.14) | data formatting | bytes 2048

commit v2 on v1

--- a/solution.py
+++ b/solution.py
@@ -78,10 +78,10 @@
     dims,
     x_hbm, wk_hbm, wv_hbm, wg_ref, bias_ref, scale_ref, spike_ref, cache_hbm, prior_hbm,
     query_ref, own_key_ref, own_value_ref, own_gate_ref, key_gain_ref, read_gain_ref,
-    new_cache_hbm, new_logc_ref, read_ref,
-    x_v, wk_v, wv_v, cache_v, prior_v, stage, send_v, recv_v, csend_v, crecv_v,
+    recv_v, new_logc_ref, read_ref,
+    x_v, wk_v, wv_v, cache_v, prior_v, stage, send_v, csend_v, crecv_v,
     expand_v, part_m, part_acc,
-    x_sem, w_sem, cache_sem, prior_sem, send_sem, recv_sem, csend_sem, crecv_sem, out_sem,
+    x_sem, w_sem, cache_sem, prior_sem, send_sem, recv_sem, csend_sem, crecv_sem,
 ):
     n, span, kv, head_dim, group, reps, chunk, sub = dims
     rows = reps * kv
@@ -104,9 +104,8 @@
     x_copy(0).start()
     wk_copy.start()
     wv_copy.start()
-
-    @pl.loop(1, n)
-    def _(i):
+    ahead = min(3, n)
+    for i in range(1, ahead):
         x_copy(i).start()
 
     barrier = pltpu.get_barrier_semaphore()
@@ -114,12 +113,6 @@
     @pl.loop(1, n)
     def _(k):
         pl.semaphore_signal(barrier, inc=1, device_id={"sp": (me + k) % n}, device_id_type=MESH)
-
-    prior_copy.start()
-
-    @pl.loop(0, chunks)
-    def _(c):
-        cache_copy(c).start()
 
     expand_v[...] = expander(sub, kv)
     bias_col = column(bias_ref[...])
@@ -129,7 +122,6 @@
         lax.broadcasted_iota(jnp.int32, (span, span), 0) <= lax.broadcasted_iota(jnp.int32, (span, span), 1),
         1.0, 0.0,
     )
-    pl.semaphore_wait(barrier, n - 1)
     wk_copy.wait()
     wv_copy.wait()
 
@@ -150,6 +142,19 @@
         k = step_pair(i, n)
         s = flip(me, k, n)
         x_copy(i).wait()
+
+        @pl.when(i + ahead < n)
+        def _():
+            x_copy(i + ahead).start()
+
+        @pl.when(i == n // 2)
+        def _():
+            prior_copy.start()
+
+            @pl.loop(0, chunks)
+            def _(c):
+                cache_copy(c).start()
+
         xb = x_v[s]
         keys = jnp.dot(xb, wk_v[...], preferred_element_type=F32)
         values = jnp.dot(xb, wv_v[...], preferred_element_type=F32)
@@ -172,6 +177,10 @@
             log_forget, upper, preferred_element_type=F32, precision=lax.Precision.HIGHEST
         )
 
+        @pl.when(i == 0)
+        def _():
+            pl.semaphore_wait(barrier, n - 1)
+
         @pl.when(k != 0)
         def _():
             block, sums = remote(i, s)
@@ -222,10 +231,6 @@
 
     block_expander = expander(span, kv)
 
-    def out_copy(b):
-        at = pl.ds(pl.multiple_of(b * span * kv, span * kv), span * kv)
-        return pltpu.make_async_copy(recv_v.at[b], new_cache_hbm.at[at], out_sem.at[b])
-
     @pl.loop(0, n)
     def _(i):
         k = step_pair(i, n)
@@ -247,7 +252,6 @@
             pltpu.make_async_copy(csend_v.at[i], crecv_v.at[b], crecv_sem.at[b]).wait()
             pltpu.make_async_copy(send_v.at[i], recv_v.at[b], recv_sem.at[b]).wait()
 
-        out_copy(b).start()
         keys = recv_v[b]
         bias = expand(repeat_rows(-crecv_v[b]), block_expander)
         s = attend(query_b, keys, bias, att_scale, kv)
@@ -294,13 +298,21 @@
     def _(i):
         k = step_pair(i, n)
         s = flip(me, k, n)
-        out_copy(s).wait()
 
         @pl.when(k != 0)
         def _():
             block, sums = remote(i, s)
             sums.wait_send()
             block.wait_send()
+
+
+def write_out(block_ref, sums_ref, read_ref, block_out, sums_out, read_out, sem):
+    pairs = ((block_ref, block_out), (sums_ref, sums_out), (read_ref, read_out))
+    copies = [pltpu.make_async_copy(a, b, sem.at[j]) for j, (a, b) in enumerate(pairs)]
+    for copy in copies:
+        copy.start()
+    for copy in copies:
+        copy.wait()
 
 
 def local(
@@ -339,12 +351,12 @@
     new_cache, new_logc, read = pl.pallas_call(
         functools.partial(kernel, (n, span, kv, head_dim, group, reps, chunk, sub)),
         out_shape=(
-            jax.ShapeDtypeStruct((n * block_rows, width), BF16),
-            jax.ShapeDtypeStruct((kv, n * span), F32),
-            jax.ShapeDtypeStruct((1, group * kv * head_dim), BF16),
+            pltpu.VMEM((n, block_rows, width), BF16),
+            pltpu.VMEM((kv, n * span), F32),
+            pltpu.VMEM((1, group * kv * head_dim), BF16),
         ),
         in_specs=[hbm, hbm, hbm, vmem, vmem, vmem, vmem, hbm, hbm] + [vmem] * 6,
-        out_specs=(hbm, vmem, vmem),
+        out_specs=(vmem, vmem, vmem),
         scratch_shapes=[
             pltpu.VMEM((n, span, model), BF16),
             pltpu.VMEM((model, kv * head_dim), BF16),
@@ -352,7 +364,6 @@
             pltpu.VMEM((past * kv, width), BF16),
             pltpu.VMEM((kv, past), F32),
             pltpu.VMEM((block_rows, width), F32),
-            pltpu.VMEM((n, block_rows, width), BF16),
             pltpu.VMEM((n, block_rows, width), BF16),
             pltpu.VMEM((n, kv, span), F32),
             pltpu.VMEM((n, kv, span), F32),
@@ -367,10 +378,9 @@
             pltpu.SemaphoreType.DMA((n,)),
             pltpu.SemaphoreType.DMA((n,)),
             pltpu.SemaphoreType.DMA((n,)),
-            pltpu.SemaphoreType.DMA((n,)),
         ],
         compiler_params=pltpu.CompilerParams(
-            collective_id=0, has_side_effects=True, vmem_limit_bytes=60 * 1024 * 1024
+            collective_id=0, has_side_effects=True, vmem_limit_bytes=61 * 1024 * 1024
         ),
     )(
         prompt_block_input,
@@ -389,6 +399,15 @@
         key_norm_gain.reshape(1, -1),
         read_norm_gain.reshape(1, -1),
     )
+    held = (new_cache, new_logc, read)
+    new_cache, new_logc, read = pl.pallas_call(
+        write_out,
+        out_shape=tuple(jax.ShapeDtypeStruct(a.shape, a.dtype) for a in held),
+        in_specs=[hbm] * 3,
+        out_specs=(hbm, hbm, hbm),
+        scratch_shapes=[pltpu.SemaphoreType.DMA((3,))],
+        compiler_params=pltpu.CompilerParams(vmem_limit_bytes=1024 * 1024),
+    )(*held)
     return (
         new_cache.reshape(1, n * span, kv, width),
         new_logc.reshape(1, kv, n * span),

time: 62.3 us -> 57.1 us (0.917)
  local copies, waits for them, and re-layouts: 5.56 us -> 0 us
    unnamed x3 -> x0, local copies, waits for them, and re-layouts: 5.56 us -> none
    pallas_call x0 -> x1, Pallas kernels: none -> 1.35 us  [local(): pl.pallas_call(write_out, out_shape=tuple((jax.ShapeDtypeStruct(a.shape,...]
    pallas_call x1, Pallas kernels: 55.8 us -> 54.9 us  [local(): pl.pallas_call(functools.partial(kernel, (n, span, kv, head_dim, group, r...]
where the time goes in v2:
time: 57.1 us; the launch traced here: 56.9 us
  Pallas kernels  56.2 us (98%)
  between operations  0.64 us (1%)
    pallas_call x1, Pallas kernels, local(): pl.pallas_call(functools.partial(kernel, (n, span, kv, head_dim, group, r...  54.9 us
    pallas_call x1, Pallas kernels, local(): pl.pallas_call(write_out, out_shape=tuple((jax.ShapeDtypeStruct(a.shape,...  1.35 us

profile of v2, /device:TPU:8, one launch (start us, length us, event | category | flops | bytes accessed | tf_op | source)
XLA Modules:
  0.0 56.9 jit_solution(22241265063731153)
XLA Ops:
  0.6 54.9 %shard_map.166 = (bf16[8,1024,128]{2,1,0:T(8,128)(2,1)S(1)}, f32[4,2048]{1,0:T(4,128)S(1)}, bf16[1,512]{1,0:T(2,128)(2,1)S(1)}) custom-call(bf16[8,256,2048]{2,1,0:T(8,128)(2,1)} %x_hbm.1, bf16[2048,256]{1,0:T(8,128)(2,1)} %wk_hbm.1, bf16[2048,256]{1,0:T(8,128)(2,1)} %wv_hbm.1, bf16[4,2048]{1,0:T(4,128)(2,1)} %wg_ref.1, f32[1,4]{1,0:T(1,128)} %bitcast.10, ...), custom_call_target="tpu_custom_call" | custom-call | tf_op jit(solution)/shard_map/pallas_call | solution.py:351
  55.5 1.4 %shard_map.167 = (bf16[8,1024,128]{2,1,0:T(8,128)(2,1)}, f32[4,2048]{1,0:T(4,128)}, bf16[1,512]{1,0:T(2,128)(2,1)}) custom-call(bf16[8,1024,128]{2,1,0:T(8,128)(2,1)S(1)} %get-tuple-element.9.block_ref, f32[4,2048]{1,0:T(4,128)S(1)} %get-tuple-element.10.sums_ref, bf16[1,512]{1,0:T(2,128)(2,1)S(1)} %get-tuple-element.11.read_ref), custom_call_target="tpu_custom_call" | custom-call | tf_op jit(solution)/shard_map/pallas_call | solution.py:403
